TPU v7x, 128 devices: a whole 4x4x4 slice. The times are simulated.
128 devices in a mesh: ep: 64 (over z, y, x), tp: 2 (over core).
Axes of the slice: x: 4, y: 4, z: 4, core: 2. Of those that a mesh axis runs over, the one named last changes fastest.
Arguments:
- tokens: bfloat16 [32768, 2048], P(('ep', 'tp')), may hold values from -6 to 6
- norm_gain: float32 [2048], replicated, may hold values from 0.1 to 1.9
- norm_bias: float32 [2048], replicated, may hold values from -3 to 3
- gate_weight: bfloat16 [64, 2048, 1024], P('ep', None, 'tp'), may hold values from -0.125 to 0.125
- up_weight: bfloat16 [64, 2048, 1024], P('ep', None, 'tp'), may hold values from -0.125 to 0.125
- down_weight: bfloat16 [64, 1024, 2048], P('ep', 'tp'), may hold values from -0.1875 to 0.1875
- expert_ids: int32 [32768, 2], P(('ep', 'tp')), may hold values from 0 to 63, all different within a row; in each aligned block of 256 rows (0 to 255, 256 to 511, ...) at most 16 rows name the same one
- route_weights: float32 [32768, 2], P(('ep', 'tp')), may hold values from 0.2 to 1
Outputs:
- mixed: bfloat16 [32768, 2048], P(('ep', 'tp'))
Inputs may be any that keep to these rules, and one draw needn't show every extreme that they name: `expert_ids`: a token's 2 experts differ; in the tokens of one device (aligned blocks of 256 rows) no expert is named by more than 16 entries, a bound that some block reaches.
All inputs are finite; a program needn't handle non-finite values.
Results may differ from a plain program's by a relative error of at most 0.0071.
Values may be sent and summed in bfloat16 or wider, within the bound.
A program may use at most 128 MiB of HBM per device.

v0:
```python
import jax
import jax.numpy as jnp
from jax import lax
from jax.sharding import PartitionSpec as P


def body(
    tokens, norm_gain, norm_bias, gate_weight, up_weight, down_weight, expert_ids, route_weights
):
    tok_rows, width = tokens.shape
    topk = expert_ids.shape[1]
    experts = lax.axis_size("ep")
    capacity = max(4 * tok_rows // experts, 4)
    values = tokens.astype(jnp.float32)
    centre = values - jnp.mean(values, axis=-1, keepdims=True)
    spread = jnp.mean(centre * centre, axis=-1, keepdims=True)
    normed = (centre * lax.rsqrt(spread + 1e-05) * norm_gain + norm_bias).astype(jnp.bfloat16)
    flat_ids = expert_ids.reshape(-1)
    onehot = (flat_ids[:, None] == jnp.arange(experts, dtype=jnp.int32)[None, :]).astype(jnp.int32)
    slot = jnp.sum(jnp.cumsum(onehot, axis=0) * onehot, axis=1) - 1
    target = flat_ids * capacity + slot
    buffer = (
        jnp.zeros((experts * capacity, width), jnp.bfloat16)
        .at[target]
        .set(jnp.repeat(normed, topk, axis=0))
    )
    buffer = buffer.reshape(experts, capacity, width)
    w_gate = gate_weight[0]
    w_up = up_weight[0]
    w_down = down_weight[0]
    rows = lax.all_to_all(buffer, "ep", split_axis=0, concat_axis=0, tiled=True)
    sources, slots, _ = rows.shape
    flat = rows.reshape(-1, width)
    pieces = lax.all_gather((w_gate, w_up), "tp", axis=1, tiled=True)
    gate = jnp.dot(flat, pieces[0], preferred_element_type=jnp.float32)
    upper = jnp.dot(flat, pieces[1], preferred_element_type=jnp.float32)
    hidden = (jax.nn.silu(gate) * upper).astype(jnp.bfloat16)
    result = jnp.dot(
        hidden, lax.all_gather(w_down, "tp", axis=0, tiled=True), preferred_element_type=jnp.float32
    ).astype(jnp.bfloat16)
    returned = lax.all_to_all(
        result.reshape(sources, slots, width), "ep", split_axis=0, concat_axis=0, tiled=True
    )
    picked = returned.reshape(-1, width)[target].astype(jnp.float32).reshape(tok_rows, topk, width)
    return jnp.sum(picked * route_weights[:, :, None], axis=1).astype(jnp.bfloat16)


def solution(mesh):
    placed = (
        P(("ep", "tp"), None),
        P(),
        P(),
        P("ep", None, "tp"),
        P("ep", None, "tp"),
        P("ep", "tp", None),
        P(("ep", "tp"), None),
        P(("ep", "tp"), None),
    )
    return jax.shard_map(
        body, mesh=mesh, in_specs=placed, out_specs=P(("ep", "tp"), None), check_vma=False
    )
```

profile of v0, /device:TPU:0, one launch (start us, length us, event | category | flops | bytes accessed | tf_op | source)
XLA Modules:
  0.0 207.6 jit_solution(8266668216036979915)
XLA Ops:
  6.5 0.0 copy-start.3
  6.5 0.0 copy-start
  6.5 0.0 copy-start.1
  6.5 0.0 copy-start.2
  6.5 0.0 all-gather.9.cloned.1.call-start
  6.6 0.7 all-gather.9.cloned.1.call-update
  7.3 0.0 all-gather.7.cloned.1.call-start
  7.3 0.7 all-gather.7.cloned.1.call-update
  8.0 0.0 copy-done.3
  8.0 0.1 copy.11
  8.2 0.1 eq.29
  8.3 0.0 copy-done
  8.4 0.2 convert_reduce_fusion
  8.6 1.2 reduce-window.6
  9.8 0.2 slice_reduce_fusion
  10.0 0.1 eq.25
  10.2 0.1 copy.10
  10.3 0.1 mul.55
  10.5 0.4 fusion.13
  10.9 0.0 copy-done.1
  10.9 0.0 copy-done.2
  10.9 0.5 fusion.16
  11.4 1.3 broadcast_in_dim.5
  12.7 2.3 %reshape.104 = bf16[512,2048]{1,0:T(8,128)(2,1)} reshape(bf16[256,2,2048]{2,1,0:T(2,128)(2,1)S(1)} %broadcast_in_dim.5) | data formatting | bytes 4194304 | tf_op jit(solution)/shard_map/reshape | solution.py:25
  15.0 0.1 fusion.20
  15.1 7.3 %scatter_custom_fusion = bf16[1024,2048]{1,0:T(8,128)(2,1)} fusion(s32[512]{0:T(512)S(1)} %bitcast.39, bf16[512,2048]{1,0:T(8,128)(2,1)} %reshape.104, bf16[]{:T(256)} %constant.9.clone.1), kind=kCustom, calls=%fused_computation.19 | custom fusion | bytes 4194816 | tf_op jit(solution)/shard_map/scatter | solution.py:25
  22.5 11.8 %all-to-all-start = ((bf16[64,16,2048]{2,1,0:T(8,128)(2,1)}), bf16[64,16,2048]{2,1,0:T(8,128)(2,1)}, u32[]{:S(2)}, u32[]{:S(2)}) async-start(bf16[64,16,2048]{2,1,0:T(8,128)(2,1)} %bitcast.37), calls=%async_computation | async-start | bytes 8388608 | tf_op jit(solution)/shard_map/all_to_all | solution.py:31
  34.3 0.2 all-gather.11.cloned.1.call-start
  34.5 0.5 all-gather.11.cloned.1.call-update
  35.0 54.5 %all-to-all-done = bf16[64,16,2048]{2,1,0:T(8,128)(2,1)} async-done(((bf16[64,16,2048]{2,1,0:T(8,128)(2,1)}), bf16[64,16,2048]{2,1,0:T(8,128)(2,1)}, u32[]{:S(2)}, u32[]{:S(2)}) %all-to-all-start) | async-done | bytes 4194336 | tf_op jit(solution)/shard_map/all_to_all | solution.py:31
  89.5 0.0 all-gather.9.cloned.1.call-done
  89.5 9.9 %fusion.2 = f32[1024,1024]{1,0:T(8,128)} fusion(bf16[1024,2048]{1,0:T(8,128)(2,1)} %bitcast.4, bf16[1,2048,1024]{2,1,0:T(8,128)(2,1)} %all-gather.9.cloned.1.call-done), kind=kOutput, calls=%fused_computation.4 | convolution fusion | flops 4294967296 | bytes 12582912 | tf_op jit(solution)/shard_map/dot_general | solution.py:36
  99.4 0.0 all-gather.7.cloned.1.call-done
  99.4 9.6 %multiply_convert_fusion = bf16[1024,1024]{1,0:T(8,128)(2,1)S(1)} fusion(f32[1024,1024]{1,0:T(8,128)} %fusion.2, bf16[1024,2048]{1,0:T(8,128)(2,1)} %bitcast.4, bf16[1,2048,1024]{2,1,0:T(8,128)(2,1)} %all-gather.7.cloned.1.call-done), kind=kOutput, calls=%fused_computation.9 | convolution fusion | flops 4301258752 | bytes 14680064 | tf_op jit(solution)/shard_map/dot_general | solution.py:35
  108.9 0.0 all-gather.11.cloned.1.call-done
  109.0 8.2 %fusion.6 = bf16[1024,2048]{1,0:T(8,128)(2,1)} fusion(bf16[1024,1024]{1,0:T(8,128)(2,1)S(1)} %multiply_convert_fusion, bf16[1,1024,2048]{2,1,0:T(8,128)(2,1)} %all-gather.11.cloned.1.call-done), kind=kOutput, calls=%fused_computation.10 | convolution fusion | flops 4297064448 | bytes 10485760 | tf_op jit(solution)/shard_map/dot_general | solution.py:38
  117.2 0.0 copy-start.4
  117.2 7.9 %all-to-all-start.1 = ((bf16[64,16,2048]{2,1,0:T(8,128)(2,1)}), bf16[64,16,2048]{2,1,0:T(8,128)(2,1)}, u32[]{:S(2)}, u32[]{:S(2)}) async-start(bf16[64,16,2048]{2,1,0:T(8,128)(2,1)} %bitcast.38), calls=%async_computation.1 | async-start | bytes 8388608 | tf_op jit(solution)/shard_map/all_to_all | solution.py:41
  125.1 0.0 copy-done.4
  125.2 0.1 copy.14
  125.3 54.8 %all-to-all-done.1 = bf16[64,16,2048]{2,1,0:T(8,128)(2,1)} async-done(((bf16[64,16,2048]{2,1,0:T(8,128)(2,1)}), bf16[64,16,2048]{2,1,0:T(8,128)(2,1)}, u32[]{:S(2)}, u32[]{:S(2)}) %all-to-all-start.1) | async-done | bytes 4194336 | tf_op jit(solution)/shard_map/all_to_all | solution.py:41
  180.1 7.1 %gather_fusion = bf16[512,2048]{1,0:T(8,128)(2,1)S(1)} fusion(bf16[1024,2048]{1,0:T(8,128)(2,1)} %bitcast.9, s32[1024]{0:T(1024)S(1)} %pad_clamp_fusion), kind=kCustom, calls=%fused_computation | custom fusion | bytes 4196352 | tf_op jit(solution)/shard_map/gather | solution.py:44
  187.2 4.0 %reshape.91 = f32[256,2,2048]{2,1,0:T(2,128)} reshape(bf16[512,2048]{1,0:T(8,128)(2,1)S(1)} %gather_fusion) | data formatting | bytes 6291456 | tf_op jit(solution)/shard_map/convert_element_type | solution.py:44
  191.2 9.9 %multiply_reduce_fusion = bf16[256,2048]{1,0:T(8,128)(2,1)} fusion(f32[256,2,2048]{2,1,0:T(2,128)} %reshape.91, f32[256,2]{1,0:T(8,128)S(1)} %copy.14), kind=kLoop, calls=%fused_computation.8 | loop fusion | flops 1572864 | bytes 5244928 | tf_op jit(solution)/shard_map/reduce_sum | solution.py:45
  (9 shorter events, 0.1 us)
Async XLA Ops:
  6.5 1.5 copy-start.3
  6.5 1.8 copy-start
  6.5 4.4 %copy-start.1 = (f32[2048]{0:T(1024)S(1)}, f32[2048]{0:T(1024)}, u32[]{:S(2)}) copy-start(f32[2048]{0:T(1024)} %param.10) | copy-start | bytes 24580
  6.5 4.4 %copy-start.2 = (f32[2048]{0:T(1024)S(1)}, f32[2048]{0:T(1024)}, u32[]{:S(2)}) copy-start(f32[2048]{0:T(1024)} %param.9) | copy-start | bytes 24580
  6.5 83.0 %all-gather.9.cloned.1.call-start = ((), (), s32[]{:S(2)}) async-start(), calls=%async_computation.3 | async-start | bytes 6291456 | tf_op jit(solution)/shard_map/all_gather | solution.py:34
  7.3 92.1 %all-gather.7.cloned.1.call-start = ((), (), s32[]{:S(2)}) async-start(), calls=%async_computation.2 | async-start | bytes 6291456 | tf_op jit(solution)/shard_map/all_gather | solution.py:34
  22.5 67.0 %all-to-all-start = ((bf16[64,16,2048]{2,1,0:T(8,128)(2,1)}), bf16[64,16,2048]{2,1,0:T(8,128)(2,1)}, u32[]{:S(2)}, u32[]{:S(2)}) async-start(bf16[64,16,2048]{2,1,0:T(8,128)(2,1)} %bitcast.37), calls=%async_computation | async-start | bytes 8388608 | tf_op jit(solution)/shard_map/all_to_all | solution.py:31
  34.3 74.7 %all-gather.11.cloned.1.call-start = ((), (), s32[]{:S(2)}) async-start(), calls=%async_computation.4 | async-start | bytes 6291456 | tf_op jit(solution)/shard_map/all_gather | solution.py:39
  117.2 7.9 %copy-start.4 = (f32[256,2]{0,1:T(2,128)S(1)}, f32[256,2]{0,1:T(2,128)}, u32[]{:S(2)}) copy-start(f32[256,2]{0,1:T(2,128)} %param.15) | copy-start | bytes 6148
  117.2 62.9 %all-to-all-start.1 = ((bf16[64,16,2048]{2,1,0:T(8,128)(2,1)}), bf16[64,16,2048]{2,1,0:T(8,128)(2,1)}, u32[]{:S(2)}, u32[]{:S(2)}) async-start(bf16[64,16,2048]{2,1,0:T(8,128)(2,1)} %bitcast.38), calls=%async_computation.1 | async-start | bytes 8388608 | tf_op jit(solution)/shard_map/all_to_all | solution.py:41
Sparse Core Ops, SparseCore 0:
  9.0 18.8 all-gather.8
  29.5 17.6 all-gather.6
  48.9 17.6 all-gather.10
where the time goes:
time: 208 us
  waiting for transfers between devices  111 us (53%)
  matrix products  27.7 us (13%)
  local copies, waits for them, and re-layouts  23.1 us (11%)
  starting transfers between devices  20 us (10%)
  between operations  13.3 us (6%)
  other arithmetic  12.4 us (6%)
    all_to_all x1, waiting for transfers between devices, body(): lax.all_to_all(result.reshape(sources, slots, width), 'ep', split_axis=0,...  54.8 us
    all_to_all x1, waiting for transfers between devices, body(): rows = lax.all_to_all(buffer, 'ep', split_axis=0, concat_axis=0, tiled=True)  54.5 us
    all_to_all x1, starting transfers between devices, body(): rows = lax.all_to_all(buffer, 'ep', split_axis=0, concat_axis=0, tiled=True)  11.8 us
    dot_general x1, matrix products, body(): upper = jnp.dot(flat, pieces[1], preferred_element_type=jnp.float32)  9.88 us
    reduce_sum x1, other arithmetic, body(): jnp.sum(picked * route_weights[:, :, None], axis=1).astype(jnp.bfloat16)  9.86 us
    dot_general x1, matrix products, body(): gate = jnp.dot(flat, pieces[0], preferred_element_type=jnp.float32)  9.55 us
    dot_general x1, matrix products, body(): jnp.dot(hidden, lax.all_gather(w_down, 'tp', axis=0, tiled=True), preferr...  8.22 us
    all_to_all x1, starting transfers between devices, body(): lax.all_to_all(result.reshape(sources, slots, width), 'ep', split_axis=0,...  7.93 us
  transfers between devices with their start and end apart: 5, of which 2 were waited for; matrix products, arithmetic and copies ran while one was open for 16% of the time, Pallas kernels for 0%

commit v1 on v0

v1 whole, which is shorter than its diff:
```python
import jax
import jax.numpy as jnp
from jax import lax
from jax.experimental import pallas as pl
from jax.experimental.pallas import tpu as pltpu
from jax.sharding import PartitionSpec as P

MESH = pl.DeviceIdType.MESH
CAP = 16
GROUPS = 4
PER = 16
F32 = jnp.float32
BF16 = jnp.bfloat16


def chip_at(place, ep, sign):
    k, j = place >> 4, place & 15
    dz, dy = j >> 2, j & 3
    dx = (k - dz - dy) & 3
    z, y, x = ep >> 4, (ep >> 2) & 3, ep & 3
    return (((z + sign * dz) & 3) << 4) | (((y + sign * dy) & 3) << 2) | ((x + sign * dx) & 3)


def kernel(
    tok, gain, bias, ids, rw, wg, wu, wd, out,
    normed, pick, send, recv, res, ret, vg, vu, vd, hid, whi, wlo, acc,
    local_sem, wsend_sem, wrecv_sem, dsend, drecv, rsend, rrecv,
):
    ep, tp = lax.axis_index("ep"), lax.axis_index("tp")
    rows, width = tok.shape
    half = wg.shape[1]
    experts = lax.axis_size("ep")

    barrier = pltpu.get_barrier_semaphore()

    def greet(i, carry):
        pl.semaphore_signal(barrier, inc=1, device_id={"ep": (ep + i) % experts, "tp": tp}, device_id_type=MESH)
        return carry

    lax.fori_loop(1, experts, greet, 0)
    pl.semaphore_signal(barrier, inc=1, device_id={"ep": ep, "tp": 1 - tp}, device_id_type=MESH)

    mine = pl.ds(pl.multiple_of(tp * half, half), half)
    pairs = ((wg, vg.at[tp]), (wu, vu.at[tp]), (wd, vd.at[mine]))
    local = [pltpu.make_async_copy(a, b, local_sem.at[n]) for n, (a, b) in enumerate(pairs)]
    shared = [
        pltpu.make_async_remote_copy(
            src_ref=a, dst_ref=b, send_sem=wsend_sem.at[n], recv_sem=wrecv_sem.at[n],
            device_id={"ep": ep, "tp": 1 - tp}, device_id_type=MESH,
        )
        for n, (a, b) in enumerate(pairs)
    ]
    for copy in local:
        copy.start()

    step = 32

    def norm(n, carry):
        at = pl.ds(pl.multiple_of(n * step, step), step)
        values = tok[at, :].astype(F32)
        centre = values - jnp.mean(values, axis=-1, keepdims=True)
        spread = jnp.mean(centre * centre, axis=-1, keepdims=True)
        normed[at, :] = (centre * lax.rsqrt(spread + 1e-05) * gain[...] + bias[...]).astype(BF16)
        return carry

    lax.fori_loop(0, rows // step, norm, 0)

    lanes = lax.broadcasted_iota(jnp.int32, (rows, 128), 1)
    first, second = ids[:, 0:1] == lanes, ids[:, 1:2] == lanes
    named = jnp.where(first | second, 1.0, 0.0)
    earlier = lax.broadcasted_iota(jnp.int32, (rows, rows), 1) < lax.broadcasted_iota(jnp.int32, (rows, rows), 0)
    count = jnp.dot(jnp.where(earlier, 1.0, 0.0).astype(BF16), named.astype(BF16), preferred_element_type=F32)
    slot = jnp.where(named > 0.0, count, -1.0)

    total = experts * CAP
    place = lax.broadcasted_iota(jnp.int32, (total, 128), 0)
    chip = chip_at(place >> 4, ep, 1)
    spread_rows = jnp.where(lax.broadcasted_iota(jnp.int32, (total, 128), 1) == chip, 1.0, 0.0).astype(BF16)
    slot_of = jnp.dot(spread_rows, slot.T.astype(BF16), preferred_element_type=F32)
    wanted = (lax.broadcasted_iota(jnp.int32, (total, rows), 0) & 15).astype(F32)
    pick[...] = jnp.where(slot_of == wanted, 1.0, 0.0).astype(BF16)

    pl.semaphore_wait(barrier, experts)
    for copy in shared:
        copy.start()

    def dispatch_copy(i):
        return pltpu.make_async_remote_copy(
            src_ref=send.at[i], dst_ref=recv.at[i], send_sem=dsend.at[i], recv_sem=drecv.at[i],
            device_id={"ep": chip_at(i, ep, 1), "tp": tp}, device_id_type=MESH,
        )

    def return_copy(i):
        return pltpu.make_async_remote_copy(
            src_ref=res.at[i], dst_ref=ret.at[i], send_sem=rsend.at[i], recv_sem=rrecv.at[i],
            device_id={"ep": chip_at(i, ep, -1), "tp": tp}, device_id_type=MESH,
        )

    def each(low, high, action):
        def run(i, carry):
            action(i)
            return carry

        lax.fori_loop(low, high, run, 0)

    def fill(k):
        chosen = pick[pl.ds(pl.multiple_of(k * PER * CAP, PER * CAP), PER * CAP), :]
        for c in range(0, width, 512):
            piece = jnp.dot(chosen, normed[:, c : c + 512], preferred_element_type=F32).astype(BF16)
            send[pl.ds(k * PER, PER), :, c : c + 512] = piece.reshape(PER, CAP, 512)

    fill(0)
    recv[0] = send[0]

    def push(k, carry):
        fill(k)
        each(jnp.maximum((k - 1) * PER, 1), k * PER, lambda i: dispatch_copy(i).start())
        return carry

    lax.fori_loop(1, GROUPS, push, 0)

    place = lax.broadcasted_iota(jnp.int32, (128, total), 1)
    chip = chip_at(place >> 4, ep, 1)
    spread_cols = jnp.where(lax.broadcasted_iota(jnp.int32, (128, total), 0) == chip, 1.0, 0.0).astype(BF16)
    each((GROUPS - 1) * PER, GROUPS * PER, lambda i: dispatch_copy(i).start())
    weight = jnp.where(first, rw[:, 0:1], 0.0) + jnp.where(second, rw[:, 1:2], 0.0)
    high = weight.astype(BF16)
    low = (weight - high.astype(F32)).astype(BF16)
    here = jnp.dot(slot.astype(BF16), spread_cols, preferred_element_type=F32) == (
        lax.broadcasted_iota(jnp.int32, (rows, total), 1) & 15
    ).astype(F32)
    whi[...] = jnp.where(here, jnp.dot(high, spread_cols, preferred_element_type=F32), 0.0).astype(BF16)
    wlo[...] = jnp.where(here, jnp.dot(low, spread_cols, preferred_element_type=F32), 0.0).astype(BF16)

    for copy in local:
        copy.wait()
    for copy in shared:
        copy.wait_recv()

    def expert(k, carry):
        each(jnp.maximum(k * PER, 1), (k + 1) * PER, lambda i: dispatch_copy(i).wait_recv())
        x = recv[pl.ds(k * PER, PER)].reshape(PER * CAP, width)
        for t in range(2):
            for c in range(0, half, 256):
                gate = jnp.dot(x, vg[t, :, c : c + 256], preferred_element_type=F32)
                upper = jnp.dot(x, vu[t, :, c : c + 256], preferred_element_type=F32)
                hid[:, t * half + c : t * half + c + 256] = (gate / (1.0 + jnp.exp(-gate)) * upper).astype(BF16)
        for c in range(0, width, 256):
            piece = jnp.dot(hid[...], vd[:, c : c + 256], preferred_element_type=F32).astype(BF16)
            res[pl.ds(k * PER, PER), :, c : c + 256] = piece.reshape(PER, CAP, 256)
        each(jnp.maximum(k * PER, 1), (k + 1) * PER, lambda i: return_copy(i).start())
        return carry

    lax.fori_loop(0, GROUPS, expert, 0)
    ret[0] = res[0]

    acc[...] = jnp.zeros_like(acc)

    def combine(k, carry):
        each(jnp.maximum(k * PER, 1), (k + 1) * PER, lambda i: return_copy(i).wait_recv())
        at = pl.ds(pl.multiple_of(k * PER * CAP, PER * CAP), PER * CAP)
        for c in range(0, width, 512):
            y = ret[pl.ds(k * PER, PER), :, c : c + 512].reshape(PER * CAP, 512)
            acc[:, c : c + 512] += jnp.dot(whi[:, at], y, preferred_element_type=F32) + jnp.dot(
                wlo[:, at], y, preferred_element_type=F32
            )
        return carry

    lax.fori_loop(0, GROUPS, combine, 0)
    out[...] = acc[...].astype(BF16)

    for copy in shared:
        copy.wait_send()
    each(1, GROUPS * PER, lambda i: dispatch_copy(i).wait_send())
    each(1, GROUPS * PER, lambda i: return_copy(i).wait_send())


def body(tokens, norm_gain, norm_bias, gate_weight, up_weight, down_weight, expert_ids, route_weights):
    rows, width = tokens.shape
    half = gate_weight.shape[2]
    experts = lax.axis_size("ep")
    total = experts * CAP
    vmem = pl.BlockSpec(memory_space=pltpu.VMEM)
    hbm = pl.BlockSpec(memory_space=pltpu.HBM)
    buffers = pltpu.VMEM((experts, CAP, width), BF16)
    copies = pltpu.SemaphoreType.DMA((experts,))
    three = pltpu.SemaphoreType.DMA((3,))
    return pl.pallas_call(
        kernel,
        name="experts",
        out_shape=jax.ShapeDtypeStruct((rows, width), BF16),
        in_specs=[vmem] * 5 + [hbm] * 3,
        out_specs=vmem,
        scratch_shapes=[
            pltpu.VMEM((rows, width), BF16),
            pltpu.VMEM((total, rows), BF16),
            buffers, buffers, buffers, buffers,
            pltpu.VMEM((2, width, half), BF16),
            pltpu.VMEM((2, width, half), BF16),
            pltpu.VMEM((2 * half, width), BF16),
            pltpu.VMEM((PER * CAP, 2 * half), BF16),
            pltpu.VMEM((rows, total), BF16),
            pltpu.VMEM((rows, total), BF16),
            pltpu.VMEM((rows, width), F32),
            three, three, three, copies, copies, copies, copies,
        ],
        compiler_params=pltpu.CompilerParams(
            collective_id=0, has_side_effects=True, vmem_limit_bytes=60 * 1024 * 1024
        ),
    )(
        tokens, norm_gain.reshape(1, width), norm_bias.reshape(1, width), expert_ids, route_weights,
        gate_weight[0], up_weight[0], down_weight[0],
    )


def solution(mesh):
    placed = (
        P(("ep", "tp"), None),
        P(),
        P(),
        P("ep", None, "tp"),
        P("ep", None, "tp"),
        P("ep", "tp", None),
        P(("ep", "tp"), None),
        P(("ep", "tp"), None),
    )
    return jax.shard_map(body, mesh=mesh, in_specs=placed, out_specs=P(("ep", "tp"), None), check_vma=False)
```

time: 208 us -> 128 us (0.62)
  Pallas kernels: 0 us -> 122 us
  waiting for transfers between devices: 111 us -> 0 us
  matrix products: 27.7 us -> 0 us
  starting transfers between devices: 20 us -> 0 us
  local copies, waits for them, and re-layouts: 23.1 us -> 5.24 us
  between operations: 13.3 us -> 0.01 us
  other arithmetic: 12.4 us -> 0 us
    pallas_call x0 -> x1, Pallas kernels: none -> 122 us  [body(): pl.pallas_call(kernel, name='experts', out_shape=jax.ShapeDtypeStruct((ro...]
    all_to_all x2 -> x0, waiting for transfers between devices: 109 us -> none  [the longest x1 54.8 us: body(): lax.all_to_all(result.reshape(sources, slots, width), 'ep', split_axis=0,...]
    dot_general x3 -> x0, matrix products: 27.7 us -> none  [the longest x1 9.88 us: body(): upper = jnp.dot(flat, pieces[1], preferred_element_type=jnp.float32)]
    all_to_all x2 -> x0, starting transfers between devices: 19.7 us -> none  [the longest x1 11.8 us: body(): rows = lax.all_to_all(buffer, 'ep', split_axis=0, concat_axis=0, tiled=True)]
    reduce_sum x4 -> x0, other arithmetic: 10.6 us -> none  [the longest x1 9.86 us: body(): jnp.sum(picked * route_weights[:, :, None], axis=1).astype(jnp.bfloat16)]
    scatter x1 -> x0, local copies, waits for them, and re-layouts: 7.34 us -> none  [body(): buffer = jnp.zeros((experts * capacity, width), jnp.bfloat16).at[target]....]
    gather x1 -> x0, local copies, waits for them, and re-layouts: 7.13 us -> none  [body(): returned.reshape(-1, width)[target].astype(jnp.float32)]
    unnamed x12 -> x3, local copies, waits for them, and re-layouts: 0.28 us -> 5.24 us
  transfers between devices with their start and end apart: 5 -> 0, of which waited for: 2 -> 0; matrix products, arithmetic and copies ran while one was open for 16% -> 0% of each run, Pallas kernels for 0% -> 0%
where the time goes in v1:
time: 128 us; the launch traced here: 127 us
  Pallas kernels  122 us (95%)
  local copies, waits for them, and re-layouts  5.24 us (4%)
    pallas_call x1, Pallas kernels, body(): pl.pallas_call(kernel, name='experts', out_shape=jax.ShapeDtypeStruct((ro...  122 us
    unnamed x3, local copies, waits for them, and re-layouts  5.24 us

profile of v1, /device:TPU:0, one launch (start us, length us, event | category | flops | bytes accessed | tf_op | source)
XLA Modules:
  0.0 126.9 jit_solution(2530890431970275918)
XLA Ops:
  0.0 1.5 %copy.9.ids = s32[256,2]{1,0:T(8,128)} copy(s32[256,2]{0,1:T(2,128)} %param.14) | data formatting | bytes 4096 | tf_op args[6]
  1.5 1.5 %copy.10.rw = f32[256,2]{1,0:T(8,128)} copy(f32[256,2]{0,1:T(2,128)} %param.15) | data formatting | bytes 4096 | tf_op args[7]
  2.9 121.7 %experts.1 = bf16[256,2048]{1,0:T(8,128)(2,1)} custom-call(bf16[256,2048]{1,0:T(8,128)(2,1)} %tok.1, f32[1,2048]{1,0:T(1,128)} %bitcast.8, f32[1,2048]{1,0:T(1,128)} %bitcast.9, s32[256,2]{1,0:T(8,128)} %copy.9.ids, f32[256,2]{1,0:T(8,128)} %copy.10.rw, bf16[2048,512]{1,0:T(8,128)(2,1)} %bitcast.5, bf16[2048,512]{1,0:T(8,128)(2,1)} %bitcast.6, ...), custom_call_target="tpu_custom_call" | custom-call | tf_op jit(solution)/shard_map/experts/pallas_call | solution.py:188
  124.6 2.3 %copy.12 = bf16[256,2048]{1,0:T(8,128)(2,1)} copy(bf16[256,2048]{1,0:T(8,128)(2,1)} %experts.1) | data formatting | bytes 2097152

commit v2 on v1

v2 whole, which is shorter than its diff:
```python
import jax
import jax.numpy as jnp
from jax import lax
from jax.experimental import pallas as pl
from jax.experimental.pallas import tpu as pltpu
from jax.sharding import PartitionSpec as P

MESH = pl.DeviceIdType.MESH
CAP = 16
GROUPS = 8
PER = 64 // GROUPS
F32 = jnp.float32
BF16 = jnp.bfloat16
PLACES = (
    0o000, 0o332, 0o221, 0o113, 0o211, 0o313, 0o131, 0o033,
    0o321, 0o213, 0o331, 0o123, 0o311, 0o133, 0o001, 0o103,
    0o230, 0o300, 0o112, 0o121, 0o323, 0o032, 0o011, 0o203,
    0o010, 0o320, 0o122, 0o101, 0o223, 0o002, 0o301, 0o233,
    0o120, 0o020, 0o200, 0o322, 0o201, 0o003, 0o132, 0o312,
    0o110, 0o330, 0o222, 0o111, 0o333, 0o102, 0o021, 0o303,
    0o210, 0o220, 0o100, 0o232, 0o031, 0o013, 0o022, 0o302,
    0o030, 0o310, 0o130, 0o212, 0o231, 0o023, 0o202, 0o012,
)


def kernel(
    tok, small, wg, wu, wd, out,
    rows_in,
    normed, spread, pick, send, recv, res, ret, vg, vu, vd, hid, whi, wlo, acc,
    in_sem, local_sem, wsend_sem, wrecv_sem, dsend, drecv, rsend, rrecv,
):
    ep, tp = lax.axis_index("ep"), lax.axis_index("tp")
    rows, width = tok.shape
    half = wg.shape[1]
    experts = lax.axis_size("ep")
    z, y, x = ep >> 4, (ep >> 2) & 3, ep & 3
    ahead = [[((at + d) & 3) << shift for d in range(4)] for at, shift in ((z, 4), (y, 2), (x, 0))]
    behind = [[((at - d) & 3) << shift for d in range(4)] for at, shift in ((z, 4), (y, 2), (x, 0))]

    def chip_at(i, steps):
        place = PLACES[i]
        return steps[0][place >> 6] | steps[1][(place >> 3) & 7] | steps[2][place & 7]

    block = rows // 4
    token_rows = [
        pltpu.make_async_copy(tok.at[pl.ds(n * block, block)], rows_in.at[pl.ds(n * block, block)], in_sem.at[n])
        for n in range(4)
    ]
    for copy in token_rows:
        copy.start()

    barrier = pltpu.get_barrier_semaphore()

    def greet(i, carry):
        pl.semaphore_signal(barrier, inc=1, device_id={"ep": (ep + i) & (experts - 1), "tp": tp}, device_id_type=MESH)
        return carry

    pl.semaphore_signal(barrier, inc=1, device_id={"ep": ep, "tp": 1 - tp}, device_id_type=MESH)
    with jax.named_scope("s_greet"):
        lax.fori_loop(1, experts, greet, 0)

    mine = pl.ds(pl.multiple_of(tp * half, half), half)
    pairs = ((wg, vg.at[tp]), (wu, vu.at[tp]), (wd, vd.at[mine]))
    local = [pltpu.make_async_copy(a, b, local_sem.at[n]) for n, (a, b) in enumerate(pairs)]
    shared = [
        pltpu.make_async_remote_copy(
            src_ref=a, dst_ref=b, send_sem=wsend_sem.at[n], recv_sem=wrecv_sem.at[n],
            device_id={"ep": ep, "tp": 1 - tp}, device_id_type=MESH,
        )
        for n, (a, b) in enumerate(pairs)
    ]

    with jax.named_scope("s_route"):
        later = lax.broadcasted_iota(jnp.int32, (rows, rows), 0) < lax.broadcasted_iota(jnp.int32, (rows, rows), 1)
        later = jnp.where(later, 1.0, 0.0).astype(BF16)
        total = experts * CAP
        lanes = lax.broadcasted_iota(jnp.int32, (CAP, 128), 1)
        for i in range(experts):
            spread[i * CAP : (i + 1) * CAP, :] = jnp.where(lanes == chip_at(i, ahead), 1.0, 0.0).astype(BF16)
        expert_rows = lax.broadcasted_iota(jnp.int32, (128, rows), 0).astype(F32)
        first, second = small[0:1, width : width + rows] == expert_rows, small[1:2, width : width + rows] == expert_rows
        named = first | second
        count = jnp.dot(jnp.where(named, 1.0, 0.0).astype(BF16), later, preferred_element_type=F32)
        slot = jnp.where(named, count, -1.0)
        slot_of = jnp.dot(spread[...], slot.astype(BF16), preferred_element_type=F32)
        wanted = (lax.broadcasted_iota(jnp.int32, (total, rows), 0) & 15).astype(F32)
        pick[...] = jnp.where(slot_of == wanted, 1.0, 0.0).astype(BF16)

    with jax.named_scope("s_ln"):
        step = 32

        def norm(n, carry):
            at = pl.ds(pl.multiple_of(n * step, step), step)
            values = rows_in[at, :].astype(F32)
            centre = values - jnp.mean(values, axis=-1, keepdims=True)
            spread = jnp.mean(centre * centre, axis=-1, keepdims=True)
            normed[at, :] = (centre * lax.rsqrt(spread + 1e-05) * small[0:1, 0:width] + small[1:2, 0:width]).astype(BF16)
            return carry

        for copy in token_rows:
            copy.wait()
        lax.fori_loop(0, rows // step, norm, 0)

    def dispatch_copy(i):
        return pltpu.make_async_remote_copy(
            src_ref=send.at[i], dst_ref=recv.at[i], send_sem=dsend.at[i], recv_sem=drecv.at[i],
            device_id={"ep": chip_at(i, ahead), "tp": tp}, device_id_type=MESH,
        )

    def return_copy(i):
        return pltpu.make_async_remote_copy(
            src_ref=res.at[i], dst_ref=ret.at[i], send_sem=rsend.at[i], recv_sem=rrecv.at[i],
            device_id={"ep": chip_at(i, behind), "tp": tp}, device_id_type=MESH,
        )

    def members(k, action):
        for g in range(GROUPS):

            @pl.when(k == g)
            def _():
                for i in range(max(g * PER, 1), (g + 1) * PER):
                    action(i)

    def fill(k):
        chosen = pick[pl.ds(pl.multiple_of(k * PER * CAP, PER * CAP), PER * CAP), :]
        for c in range(0, width, 512):
            piece = jnp.dot(chosen, normed[:, c : c + 512], preferred_element_type=F32).astype(BF16)
            send[pl.ds(k * PER, PER), :, c : c + 512] = piece.reshape(PER, CAP, 512)

    fill(0)
    with jax.named_scope("s_bar"):
        pl.semaphore_wait(barrier, experts)
    for i in range(1, PER):
        dispatch_copy(i).start()
    for copy in shared:
        copy.start()
    for copy in local:
        copy.start()
    recv[0] = send[0]

    with jax.named_scope("s_push"):
        for k in range(1, GROUPS):
            fill(k)
            for i in range(k * PER, (k + 1) * PER):
                dispatch_copy(i).start()

    def to_rows(v):
        return lax.dot_general(v, spread[...], (((1,), (1,)), ((), ())), preferred_element_type=F32)

    weight = (jnp.where(first, small[0:1, width + rows : width + 2 * rows], 0.0) + jnp.where(second, small[1:2, width + rows : width + 2 * rows], 0.0)).T
    high = weight.astype(BF16)
    low = (weight - high.astype(F32)).astype(BF16)
    here = to_rows(slot.T.astype(BF16)) == (
        lax.broadcasted_iota(jnp.int32, (rows, total), 1) & 15
    ).astype(F32)
    whi[...] = jnp.where(here, to_rows(high), 0.0).astype(BF16)
    wlo[...] = jnp.where(here, to_rows(low), 0.0).astype(BF16)
    acc[...] = jnp.zeros_like(acc)

    with jax.named_scope("s_wwait"):
        for copy in local:
            copy.wait()
        for copy in shared:
            copy.wait_recv()

    def expert(k, carry):
        with jax.named_scope("s_dwait"):
            members(k, lambda i: dispatch_copy(i).wait_recv())
        x = recv[pl.ds(k * PER, PER)].reshape(PER * CAP, width)
        for t in range(2):
            for c in range(0, half, 256):
                gate = jnp.dot(x, vg[t, :, c : c + 256], preferred_element_type=F32)
                upper = jnp.dot(x, vu[t, :, c : c + 256], preferred_element_type=F32)
                hid[:, t * half + c : t * half + c + 256] = (gate / (1.0 + jnp.exp(-gate)) * upper).astype(BF16)
        for c in range(0, width, 256):
            piece = jnp.dot(hid[...], vd[:, c : c + 256], preferred_element_type=F32).astype(BF16)
            res[pl.ds(k * PER, PER), :, c : c + 256] = piece.reshape(PER, CAP, 256)
        with jax.named_scope("s_rsend"):
            members(k, lambda i: return_copy(i).start())
        return carry

    lax.fori_loop(0, GROUPS, expert, 0)
    ret[0] = res[0]

    def combine(k, carry):
        with jax.named_scope("s_rwait"):
            members(k, lambda i: return_copy(i).wait_recv())
        at = pl.ds(pl.multiple_of(k * PER * CAP, PER * CAP), PER * CAP)
        for c in range(0, width, 512):
            y = ret[pl.ds(k * PER, PER), :, c : c + 512].reshape(PER * CAP, 512)
            acc[:, c : c + 512] += jnp.dot(whi[:, at], y, preferred_element_type=F32) + jnp.dot(
                wlo[:, at], y, preferred_element_type=F32
            )
        return carry

    lax.fori_loop(0, GROUPS, combine, 0)
    with jax.named_scope("s_out"):
        out[...] = acc[...].astype(BF16)

    with jax.named_scope("s_end"):
        for copy in shared:
            copy.wait_send()
        for i in range(1, experts):
            dispatch_copy(i).wait_send()
            return_copy(i).wait_send()


def body(tokens, norm_gain, norm_bias, gate_weight, up_weight, down_weight, expert_ids, route_weights):
    rows, width = tokens.shape
    half = gate_weight.shape[2]
    experts = lax.axis_size("ep")
    total = experts * CAP
    small = jnp.concatenate((jnp.stack((norm_gain, norm_bias)), expert_ids.T.astype(F32), route_weights.T), axis=1)
    hbm = pl.BlockSpec(memory_space=pltpu.HBM)
    buffers = pltpu.VMEM((experts, CAP, width), BF16)
    copies = pltpu.SemaphoreType.DMA((experts,))
    three = pltpu.SemaphoreType.DMA((3,))
    return pl.pallas_call(
        kernel,
        name="experts",
        out_shape=jax.ShapeDtypeStruct((rows, width), BF16),
        in_specs=[hbm, pl.BlockSpec(memory_space=pltpu.VMEM), hbm, hbm, hbm],
        out_specs=pl.BlockSpec(memory_space=pltpu.VMEM),
        scratch_shapes=[
            pltpu.VMEM((rows, width), BF16),
            pltpu.VMEM((rows, width), BF16),
            pltpu.VMEM((total, 128), BF16),
            pltpu.VMEM((total, rows), BF16),
            buffers, buffers, buffers, buffers,
            pltpu.VMEM((2, width, half), BF16),
            pltpu.VMEM((2, width, half), BF16),
            pltpu.VMEM((2 * half, width), BF16),
            pltpu.VMEM((PER * CAP, 2 * half), BF16),
            pltpu.VMEM((rows, total), BF16),
            pltpu.VMEM((rows, total), BF16),
            pltpu.VMEM((rows, width), F32),
            pltpu.SemaphoreType.DMA((4,)),
            three, three, three, copies, copies, copies, copies,
        ],
        compiler_params=pltpu.CompilerParams(
            collective_id=0, has_side_effects=True, vmem_limit_bytes=52 * 1024 * 1024
        ),
    )(
        tokens, small,
        gate_weight[0], up_weight[0], down_weight[0],
    )


def solution(mesh):
    placed = (
        P(("ep", "tp"), None),
        P(),
        P(),
        P("ep", None, "tp"),
        P("ep", None, "tp"),
        P("ep", "tp", None),
        P(("ep", "tp"), None),
        P(("ep", "tp"), None),
    )
    return jax.shard_map(body, mesh=mesh, in_specs=placed, out_specs=P(("ep", "tp"), None), check_vma=False)
```

time: 128 us -> 120 us (0.938)
  the two profiles are of different devices: /device:TPU:0 before, /device:TPU:6 now
where the time goes in v2:
time: 120 us
  Pallas kernels  118 us (98%)
  other arithmetic  1.43 us (1%)
    pallas_call x1, Pallas kernels, body(): pl.pallas_call(kernel, name='experts', out_shape=jax.ShapeDtypeStruct((ro...  118 us

profile of v2, /device:TPU:6, one launch (start us, length us, event | category | flops | bytes accessed | tf_op | source)
XLA Modules:
  0.0 120.0 jit_solution(4420773394331141714)
XLA Ops:
  0.0 0.7 convert_bitcast_fusion
  0.7 0.7 pad_maximum_fusion.small
  1.4 117.6 %experts.1 = bf16[256,2048]{1,0:T(8,128)(2,1)S(1)} custom-call(bf16[256,2048]{1,0:T(8,128)(2,1)} %tok.1, f32[2,2560]{1,0:T(2,128)S(1)} %pad_maximum_fusion.small, bf16[2048,512]{1,0:T(8,128)(2,1)} %bitcast.8, bf16[2048,512]{1,0:T(8,128)(2,1)} %bitcast.9, bf16[512,2048]{1,0:T(8,128)(2,1)} %bitcast.10), custom_call_target="tpu_custom_call" | custom-call | tf_op jit(solution)/shard_map/experts/pallas_call | solution.py:218
  119.0 1.0 copy.10

commit v3 on v2

--- a/solution.py
+++ b/solution.py
@@ -12,20 +12,20 @@
 F32 = jnp.float32
 BF16 = jnp.bfloat16
 PLACES = (
-    0o000, 0o332, 0o221, 0o113, 0o211, 0o313, 0o131, 0o033,
-    0o321, 0o213, 0o331, 0o123, 0o311, 0o133, 0o001, 0o103,
-    0o230, 0o300, 0o112, 0o121, 0o323, 0o032, 0o011, 0o203,
-    0o010, 0o320, 0o122, 0o101, 0o223, 0o002, 0o301, 0o233,
-    0o120, 0o020, 0o200, 0o322, 0o201, 0o003, 0o132, 0o312,
-    0o110, 0o330, 0o222, 0o111, 0o333, 0o102, 0o021, 0o303,
-    0o210, 0o220, 0o100, 0o232, 0o031, 0o013, 0o022, 0o302,
-    0o030, 0o310, 0o130, 0o212, 0o231, 0o023, 0o202, 0o012,
+    0o000, 0o121, 0o202, 0o323, 0o112, 0o233, 0o310, 0o031,
+    0o220, 0o301, 0o022, 0o103, 0o332, 0o013, 0o130, 0o211,
+    0o001, 0o122, 0o203, 0o320, 0o113, 0o230, 0o311, 0o032,
+    0o221, 0o302, 0o023, 0o100, 0o333, 0o010, 0o131, 0o212,
+    0o002, 0o123, 0o200, 0o321, 0o110, 0o231, 0o312, 0o033,
+    0o222, 0o303, 0o020, 0o101, 0o330, 0o011, 0o132, 0o213,
+    0o003, 0o120, 0o201, 0o322, 0o111, 0o232, 0o313, 0o030,
+    0o223, 0o300, 0o021, 0o102, 0o331, 0o012, 0o133, 0o210,
 )
 
 
 def kernel(
-    tok, small, wg, wu, wd, out,
-    rows_in,
+    tok, gain, bias, ids, rw, wg, wu, wd, out,
+    rows_in, gain_in, bias_in, ids_in, rw_in,
     normed, spread, pick, send, recv, res, ret, vg, vu, vd, hid, whi, wlo, acc,
     in_sem, local_sem, wsend_sem, wrecv_sem, dsend, drecv, rsend, rrecv,
 ):
@@ -42,11 +42,15 @@
         return steps[0][place >> 6] | steps[1][(place >> 3) & 7] | steps[2][place & 7]
 
     block = rows // 4
+    inputs = [
+        pltpu.make_async_copy(a, b, in_sem.at[n])
+        for n, (a, b) in enumerate(((ids, ids_in), (rw, rw_in), (gain, gain_in), (bias, bias_in)))
+    ]
     token_rows = [
-        pltpu.make_async_copy(tok.at[pl.ds(n * block, block)], rows_in.at[pl.ds(n * block, block)], in_sem.at[n])
+        pltpu.make_async_copy(tok.at[pl.ds(n * block, block)], rows_in.at[pl.ds(n * block, block)], in_sem.at[4 + n])
         for n in range(4)
     ]
-    for copy in token_rows:
+    for copy in inputs + token_rows:
         copy.start()
 
     barrier = pltpu.get_barrier_semaphore()
@@ -77,8 +81,10 @@
         lanes = lax.broadcasted_iota(jnp.int32, (CAP, 128), 1)
         for i in range(experts):
             spread[i * CAP : (i + 1) * CAP, :] = jnp.where(lanes == chip_at(i, ahead), 1.0, 0.0).astype(BF16)
-        expert_rows = lax.broadcasted_iota(jnp.int32, (128, rows), 0).astype(F32)
-        first, second = small[0:1, width : width + rows] == expert_rows, small[1:2, width : width + rows] == expert_rows
+        for copy in inputs:
+            copy.wait()
+        expert_rows = lax.broadcasted_iota(jnp.int32, (128, rows), 0)
+        first, second = ids_in[0:1, :] == expert_rows, ids_in[1:2, :] == expert_rows
         named = first | second
         count = jnp.dot(jnp.where(named, 1.0, 0.0).astype(BF16), later, preferred_element_type=F32)
         slot = jnp.where(named, count, -1.0)
@@ -94,7 +100,7 @@
             values = rows_in[at, :].astype(F32)
             centre = values - jnp.mean(values, axis=-1, keepdims=True)
             spread = jnp.mean(centre * centre, axis=-1, keepdims=True)
-            normed[at, :] = (centre * lax.rsqrt(spread + 1e-05) * small[0:1, 0:width] + small[1:2, 0:width]).astype(BF16)
+            normed[at, :] = (centre * lax.rsqrt(spread + 1e-05) * gain_in[...] + bias_in[...]).astype(BF16)
             return carry
 
         for copy in token_rows:
@@ -147,7 +153,7 @@
     def to_rows(v):
         return lax.dot_general(v, spread[...], (((1,), (1,)), ((), ())), preferred_element_type=F32)
 
-    weight = (jnp.where(first, small[0:1, width + rows : width + 2 * rows], 0.0) + jnp.where(second, small[1:2, width + rows : width + 2 * rows], 0.0)).T
+    weight = (jnp.where(first, rw_in[0:1, :], 0.0) + jnp.where(second, rw_in[1:2, :], 0.0)).T
     high = weight.astype(BF16)
     low = (weight - high.astype(F32)).astype(BF16)
     here = to_rows(slot.T.astype(BF16)) == (
@@ -210,7 +216,6 @@
     half = gate_weight.shape[2]
     experts = lax.axis_size("ep")
     total = experts * CAP
-    small = jnp.concatenate((jnp.stack((norm_gain, norm_bias)), expert_ids.T.astype(F32), route_weights.T), axis=1)
     hbm = pl.BlockSpec(memory_space=pltpu.HBM)
     buffers = pltpu.VMEM((experts, CAP, width), BF16)
     copies = pltpu.SemaphoreType.DMA((experts,))
@@ -219,10 +224,14 @@
         kernel,
         name="experts",
         out_shape=jax.ShapeDtypeStruct((rows, width), BF16),
-        in_specs=[hbm, pl.BlockSpec(memory_space=pltpu.VMEM), hbm, hbm, hbm],
+        in_specs=[hbm] * 8,
         out_specs=pl.BlockSpec(memory_space=pltpu.VMEM),
         scratch_shapes=[
             pltpu.VMEM((rows, width), BF16),
+            pltpu.VMEM((1, width), F32),
+            pltpu.VMEM((1, width), F32),
+            pltpu.VMEM((2, rows), jnp.int32),
+            pltpu.VMEM((2, rows), F32),
             pltpu.VMEM((rows, width), BF16),
             pltpu.VMEM((total, 128), BF16),
             pltpu.VMEM((total, rows), BF16),
@@ -234,16 +243,19 @@
             pltpu.VMEM((rows, total), BF16),
             pltpu.VMEM((rows, total), BF16),
             pltpu.VMEM((rows, width), F32),
-            pltpu.SemaphoreType.DMA((4,)),
+            pltpu.SemaphoreType.DMA((8,)),
             three, three, three, copies, copies, copies, copies,
         ],
         compiler_params=pltpu.CompilerParams(
             collective_id=0, has_side_effects=True, vmem_limit_bytes=52 * 1024 * 1024
         ),
-    )(
-        tokens, small,
-        gate_weight[0], up_weight[0], down_weight[0],
-    )
+    )(*(
+        pltpu.with_memory_space_constraint(array, pltpu.HBM)
+        for array in (
+            tokens, norm_gain.reshape(1, width), norm_bias.reshape(1, width), expert_ids.T, route_weights.T,
+            gate_weight[0], up_weight[0], down_weight[0],
+        )
+    ))
 
 
 def solution(mesh):

time: 120 us -> 108 us (0.900)
  the two profiles are of different devices: /device:TPU:6 before, /device:TPU:0 now
where the time goes in v3:
time: 108 us; the launch traced here: 107 us
  Pallas kernels  106 us (98%)
    pallas_call x1, Pallas kernels, body(): pl.pallas_call(kernel, name='experts', out_shape=jax.ShapeDtypeStruct((ro...  106 us

profile of v3, /device:TPU:0, one launch (start us, length us, event | category | flops | bytes accessed | tf_op | source)
XLA Modules:
  0.0 107.0 jit_solution(8823268827598739733)
XLA Ops:
  0.0 106.1 %experts.1 = bf16[256,2048]{1,0:T(8,128)(2,1)S(1)} custom-call(bf16[256,2048]{1,0:T(8,128)(2,1)} %tok.1, f32[1,2048]{1,0:T(1,128)} %bitcast.10, f32[1,2048]{1,0:T(1,128)} %bitcast.11, s32[2,256]{1,0:T(2,128)} %bitcast.12, f32[2,256]{1,0:T(2,128)} %bitcast.13, bf16[2048,512]{1,0:T(8,128)(2,1)} %bitcast.7, bf16[2048,512]{1,0:T(8,128)(2,1)} %bitcast.8, ...), custom_call_target="tpu_custom_call" | custom-call | tf_op jit(solution)/shard_map/experts/pallas_call | solution.py:223
  106.1 1.0 copy.10

commit v4 on v3

--- a/solution.py
+++ b/solution.py
@@ -23,6 +23,14 @@
 )
 
 
+def hops(i):
+    digits = (PLACES[i] >> 6, (PLACES[i] >> 3) & 7, PLACES[i] & 7)
+    return sum(min(d, 4 - d) for d in digits)
+
+
+FARTHEST = sorted(range(1, 64), key=lambda i: -hops(i))
+
+
 def kernel(
     tok, gain, bias, ids, rw, wg, wu, wd, out,
     rows_in, gain_in, bias_in, ids_in, rw_in,
@@ -55,13 +63,12 @@
 
     barrier = pltpu.get_barrier_semaphore()
 
-    def greet(i, carry):
-        pl.semaphore_signal(barrier, inc=1, device_id={"ep": (ep + i) & (experts - 1), "tp": tp}, device_id_type=MESH)
-        return carry
-
-    pl.semaphore_signal(barrier, inc=1, device_id={"ep": ep, "tp": 1 - tp}, device_id_type=MESH)
-    with jax.named_scope("s_greet"):
-        lax.fori_loop(1, experts, greet, 0)
+    def greet(chip, core):
+        pl.semaphore_signal(barrier, inc=1, device_id={"ep": chip, "tp": core}, device_id_type=MESH)
+
+    for i in FARTHEST:
+        greet(chip_at(i, ahead), tp)
+    greet(ep, 1 - tp)
 
     mine = pl.ds(pl.multiple_of(tp * half, half), half)
     pairs = ((wg, vg.at[tp]), (wu, vu.at[tp]), (wd, vd.at[mine]))
@@ -188,26 +195,33 @@
     lax.fori_loop(0, GROUPS, expert, 0)
     ret[0] = res[0]
 
+    for i in range(1, experts):
+        dispatch_copy(i).wait_send()
+
+    def part(k, c):
+        at = pl.ds(pl.multiple_of(k * PER * CAP, PER * CAP), PER * CAP)
+        y = ret[pl.ds(k * PER, PER), :, c : c + 512].reshape(PER * CAP, 512)
+        return jnp.dot(whi[:, at], y, preferred_element_type=F32) + jnp.dot(wlo[:, at], y, preferred_element_type=F32)
+
     def combine(k, carry):
         with jax.named_scope("s_rwait"):
             members(k, lambda i: return_copy(i).wait_recv())
-        at = pl.ds(pl.multiple_of(k * PER * CAP, PER * CAP), PER * CAP)
         for c in range(0, width, 512):
-            y = ret[pl.ds(k * PER, PER), :, c : c + 512].reshape(PER * CAP, 512)
-            acc[:, c : c + 512] += jnp.dot(whi[:, at], y, preferred_element_type=F32) + jnp.dot(
-                wlo[:, at], y, preferred_element_type=F32
-            )
+            acc[:, c : c + 512] += part(k, c)
         return carry
 
-    lax.fori_loop(0, GROUPS, combine, 0)
+    lax.fori_loop(0, GROUPS - 1, combine, 0)
+    with jax.named_scope("s_rlast"):
+        for i in range((GROUPS - 1) * PER, GROUPS * PER):
+            return_copy(i).wait_recv()
     with jax.named_scope("s_out"):
-        out[...] = acc[...].astype(BF16)
+        for c in range(0, width, 512):
+            out[:, c : c + 512] = (acc[:, c : c + 512] + part(GROUPS - 1, c)).astype(BF16)
 
     with jax.named_scope("s_end"):
         for copy in shared:
             copy.wait_send()
         for i in range(1, experts):
-            dispatch_copy(i).wait_send()
             return_copy(i).wait_send()
 
 

time: 108 us -> 107 us (level)
  no operation moved by 1% of the time
where the time goes in v4:
time: 107 us
  Pallas kernels  106 us (99%)
    pallas_call x1, Pallas kernels, body(): pl.pallas_call(kernel, name='experts', out_shape=jax.ShapeDtypeStruct((ro...  106 us

profile of v4, /device:TPU:0, one launch (start us, length us, event | category | flops | bytes accessed | tf_op | source)
XLA Modules:
  0.0 106.6 jit_solution(1023921397350267934)
XLA Ops:
  0.0 105.6 %experts.1 = bf16[256,2048]{1,0:T(8,128)(2,1)S(1)} custom-call(bf16[256,2048]{1,0:T(8,128)(2,1)} %tok.1, f32[1,2048]{1,0:T(1,128)} %bitcast.10, f32[1,2048]{1,0:T(1,128)} %bitcast.11, s32[2,256]{1,0:T(2,128)} %bitcast.12, f32[2,256]{1,0:T(2,128)} %bitcast.13, bf16[2048,512]{1,0:T(8,128)(2,1)} %bitcast.7, bf16[2048,512]{1,0:T(8,128)(2,1)} %bitcast.8, ...), custom_call_target="tpu_custom_call" | custom-call | tf_op jit(solution)/shard_map/experts/pallas_call | solution.py:237
  105.6 1.0 copy.10

commit v5 on v4

--- a/solution.py
+++ b/solution.py
@@ -34,7 +34,7 @@
 def kernel(
     tok, gain, bias, ids, rw, wg, wu, wd, out,
     rows_in, gain_in, bias_in, ids_in, rw_in,
-    normed, spread, pick, send, recv, res, ret, vg, vu, vd, hid, whi, wlo, acc,
+    normed, spread, pick, send, recv, res, ret, vg, vu, vd, hid, whi, wlo, wend, acc,
     in_sem, local_sem, wsend_sem, wrecv_sem, dsend, drecv, rsend, rrecv,
 ):
     ep, tp = lax.axis_index("ep"), lax.axis_index("tp")
@@ -145,8 +145,6 @@
         pl.semaphore_wait(barrier, experts)
     for i in range(1, PER):
         dispatch_copy(i).start()
-    for copy in shared:
-        copy.start()
     for copy in local:
         copy.start()
     recv[0] = send[0]
@@ -156,6 +154,9 @@
             fill(k)
             for i in range(k * PER, (k + 1) * PER):
                 dispatch_copy(i).start()
+
+    for copy in shared:
+        copy.start()
 
     def to_rows(v):
         return lax.dot_general(v, spread[...], (((1,), (1,)), ((), ())), preferred_element_type=F32)
@@ -169,6 +170,8 @@
     whi[...] = jnp.where(here, to_rows(high), 0.0).astype(BF16)
     wlo[...] = jnp.where(here, to_rows(low), 0.0).astype(BF16)
     acc[...] = jnp.zeros_like(acc)
+    tail = pl.ds(total - PER * CAP // 2, PER * CAP // 2)
+    wend[...] = jnp.concatenate((whi[:, tail], wlo[:, tail]), axis=1)
 
     with jax.named_scope("s_wwait"):
         for copy in local:
@@ -211,12 +214,24 @@
         return carry
 
     lax.fori_loop(0, GROUPS - 1, combine, 0)
+    cut = experts - PER // 2
+    for i in range((GROUPS - 1) * PER, cut):
+        return_copy(i).wait_recv()
+    rest = (experts - cut) * CAP
+    for c in range(0, width, 512):
+        y = ret[(GROUPS - 1) * PER : cut, :, c : c + 512].reshape(rest, 512)
+        at = pl.ds(total - 2 * rest, rest)
+        acc[:, c : c + 512] += jnp.dot(whi[:, at], y, preferred_element_type=F32) + jnp.dot(
+            wlo[:, at], y, preferred_element_type=F32
+        )
     with jax.named_scope("s_rlast"):
-        for i in range((GROUPS - 1) * PER, GROUPS * PER):
+        for i in range(cut, experts):
             return_copy(i).wait_recv()
     with jax.named_scope("s_out"):
         for c in range(0, width, 512):
-            out[:, c : c + 512] = (acc[:, c : c + 512] + part(GROUPS - 1, c)).astype(BF16)
+            y = ret[cut:experts, :, c : c + 512].reshape(rest, 512)
+            y = jnp.dot(wend[...], jnp.concatenate((y, y), axis=0), preferred_element_type=F32)
+            out[:, c : c + 512] = (acc[:, c : c + 512] + y).astype(BF16)
 
     with jax.named_scope("s_end"):
         for copy in shared:
@@ -256,6 +271,7 @@
             pltpu.VMEM((PER * CAP, 2 * half), BF16),
             pltpu.VMEM((rows, total), BF16),
             pltpu.VMEM((rows, total), BF16),
+            pltpu.VMEM((rows, PER * CAP), BF16),
             pltpu.VMEM((rows, width), F32),
             pltpu.SemaphoreType.DMA((8,)),
             three, three, three, copies, copies, copies, copies,

time: 107 us -> 108 us (level); the launches traced: 107 us -> 106 us
  no operation moved by 1% of the time
where the time goes in v5:
time: 108 us; the launch traced here: 106 us
  Pallas kernels  105 us (97%)
    pallas_call x1, Pallas kernels, body(): pl.pallas_call(kernel, name='experts', out_shape=jax.ShapeDtypeStruct((ro...  105 us

profile of v5, /device:TPU:0, one launch (start us, length us, event | category | flops | bytes accessed | tf_op | source)
XLA Modules:
  0.0 106.3 jit_solution(7534273292523837124)
XLA Ops:
  0.0 105.4 %experts.1 = bf16[256,2048]{1,0:T(8,128)(2,1)S(1)} custom-call(bf16[256,2048]{1,0:T(8,128)(2,1)} %tok.1, f32[1,2048]{1,0:T(1,128)} %bitcast.10, f32[1,2048]{1,0:T(1,128)} %bitcast.11, s32[2,256]{1,0:T(2,128)} %bitcast.12, f32[2,256]{1,0:T(2,128)} %bitcast.13, bf16[2048,512]{1,0:T(8,128)(2,1)} %bitcast.7, bf16[2048,512]{1,0:T(8,128)(2,1)} %bitcast.8, ...), custom_call_target="tpu_custom_call" | custom-call | tf_op jit(solution)/shard_map/experts/pallas_call | solution.py:252
  105.4 1.0 copy.10
